TPU v7x, 32 devices: a whole 2x2x4 slice. The times are simulated.
32 devices in a mesh: sp: 16 (over z, y, x), tp: 2 (over core).
Axes of the slice: x: 2, y: 2, z: 4, core: 2. Of those that a mesh axis runs over, the one named last changes fastest.
Arguments:
- latent: bfloat16 [4096, 2048], P(('sp', 'tp')), may hold values from -3 to 3
- context: bfloat16 [1024, 2048], P('sp'), may hold values from -6 to 6
- condition: float32 [2048], replicated, may hold values from -6 to 6
- ctx_cond: float32 [2048], replicated, may hold values from -6 to 6
- norm_gain: float32 [2048], replicated, may hold values from 0.1 to 1.9
- w_shift: bfloat16 [2048, 2048], P('sp', 'tp'), may hold values from -0.25 to 0.25
- w_scale: bfloat16 [2048, 2048], P('sp', 'tp'), may hold values from -0.25 to 0.25
- w_gate: bfloat16 [2048, 2048], P('sp', 'tp'), may hold values from -0.25 to 0.25
- w_query: bfloat16 [2048, 2048], P(None, 'tp'), may hold values from -0.125 to 0.125
- w_key: bfloat16 [2048, 2048], P(None, 'tp'), may hold values from -0.125 to 0.125
- w_value: bfloat16 [2048, 2048], P(None, 'tp'), may hold values from -0.125 to 0.125
- w_out: bfloat16 [2048, 2048], P('tp'), may hold values from -0.125 to 0.125
- rel_bias: float32 [16, 15, 31], replicated, may hold values from 2 to 250
Outputs:
- updated: bfloat16 [4096, 2048], P(('sp', 'tp'))
All inputs are finite; a program needn't handle non-finite values.
Results may differ from a plain program's by a relative error of at most 0.015.
Values may be sent and summed in bfloat16 or wider, within the bound.
A program may use at most 128 MiB of HBM per device.

v0:
```python
import jax
import jax.numpy as jnp
from jax import lax
from jax.sharding import PartitionSpec as P

HEADS = 16
HEAD_DIM = 128
GRID_W = 32
WIN_H = 8
WIN_W = 16
NORM_EPS = 1e-06
NEG_BIG = -1e30


def padded_2(cells, sides, width):
    for axis, dim in sides:
        count = lax.axis_size(axis)
        ends = count - 1
        head = lax.slice_in_dim(cells, 0, width, axis=dim)
        tail = lax.slice_in_dim(cells, cells.shape[dim] - width, cells.shape[dim], axis=dim)
        cells = jnp.concatenate(
            [
                lax.ppermute(tail, axis, [(i, (i + 1) % count) for i in range(ends)]),
                cells,
                lax.ppermute(head, axis, [((i + 1) % count, i) for i in range(ends)]),
            ],
            axis=dim,
        )
    return cells


def rms_mod(block, norm_gain, shifts, scales):
    block = block.astype(jnp.float32)
    normed = (
        block * lax.rsqrt(jnp.mean(block * block, axis=-1, keepdims=True) + NORM_EPS) * norm_gain
    )
    return (normed * (1.0 + scales) + shifts).astype(jnp.bfloat16)


def project(block, weights):
    return jnp.stack(
        [
            jnp.dot(block, weight, preferred_element_type=jnp.float32).astype(jnp.bfloat16)
            for weight in weights
        ]
    )


def on_device(
    latent,
    context,
    condition,
    ctx_cond,
    norm_gain,
    w_shift,
    w_scale,
    w_gate,
    w_query,
    w_key,
    w_value,
    w_out,
    rel_bias,
):
    tp_size = lax.axis_size("tp")
    sp_size = lax.axis_size("sp")
    head_dev = HEADS // tp_size
    head_cols = w_query.shape[1]
    model_width = w_query.shape[0]
    row_part = w_shift.shape[0]
    col_part = w_shift.shape[1]
    activated = jax.nn.silu(jnp.stack([condition, ctx_cond])).astype(jnp.bfloat16)
    act_rows = lax.dynamic_slice_in_dim(activated, lax.axis_index("sp") * row_part, row_part, 1)
    partial_value = jnp.concatenate(
        [
            jnp.dot(act_rows, w_shift, preferred_element_type=jnp.float32),
            jnp.dot(act_rows, w_scale, preferred_element_type=jnp.float32),
            jnp.dot(act_rows[:1], w_gate, preferred_element_type=jnp.float32),
        ],
        axis=0,
    )
    placed = lax.dynamic_update_slice_in_dim(
        jnp.zeros((5, model_width), jnp.float32), partial_value, lax.axis_index("tp") * col_part, 1
    )
    mod_vecs = lax.psum(placed, ("sp", "tp"))
    normed = rms_mod(latent, norm_gain, mod_vecs[0], mod_vecs[2])
    projected = project(lax.all_gather(normed, "tp", axis=0, tiled=True), (w_query, w_key, w_value))
    ctx_kv = lax.all_gather(
        project(rms_mod(context, norm_gain, mod_vecs[1], mod_vecs[3]), (w_key, w_value)),
        "sp",
        axis=1,
        tiled=True,
    )
    ctx_key3 = ctx_kv[0].reshape(-1, head_dev, HEAD_DIM)
    ctx_val3 = ctx_kv[1].reshape(-1, head_dev, HEAD_DIM)
    grid_rows = projected.shape[1] // GRID_W
    queries = projected[0].reshape(grid_rows, GRID_W, head_dev, HEAD_DIM)
    half_win = WIN_H // 2
    padded = padded_2(
        projected[1:].reshape(2, grid_rows, GRID_W, head_cols), (("sp", 1),), half_win
    )
    total_rows = grid_rows * sp_size
    first_row = lax.axis_index("sp") * grid_rows
    local_rows = jnp.arange(grid_rows, dtype=jnp.int32)
    starts = (
        jnp.clip(first_row + local_rows - half_win, 0, total_rows - WIN_H) - first_row + half_win
    )

    def take_window(start_row):
        return lax.dynamic_slice_in_dim(padded, start_row, WIN_H, 1)

    windows = jax.vmap(take_window)(starts)
    key_win = windows[:, 0].reshape(grid_rows, WIN_H, GRID_W, head_dev, HEAD_DIM)
    val_win = windows[:, 1].reshape(grid_rows, WIN_H, GRID_W, head_dev, HEAD_DIM)
    row_off = (
        starts[:, None]
        - half_win
        + jnp.arange(WIN_H, dtype=jnp.int32)[None, :]
        - local_rows[:, None]
        + WIN_H
        - 1
    )
    col_ids = jnp.arange(GRID_W, dtype=jnp.int32)
    col_start = jnp.clip(col_ids - WIN_W // 2, 0, GRID_W - WIN_W)
    col_in = (col_ids[None, :] >= col_start[:, None]) & (
        col_ids[None, :] < col_start[:, None] + WIN_W
    )
    col_off = jnp.clip(col_ids[None, :] - col_ids[:, None], 1 - WIN_W, WIN_W - 1) + WIN_W - 1
    col_hot = (col_off[:, :, None] == jnp.arange(2 * WIN_W - 1)[None, None, :]).astype(jnp.float32)
    row_hot = (row_off[:, :, None] == jnp.arange(2 * WIN_H - 1)[None, None, :]).astype(jnp.float32)
    bias_table = lax.dynamic_slice_in_dim(rel_bias, lax.axis_index("tp") * head_dev, head_dev, 0)
    col_table = jnp.einsum("hec,qwc->heqw", bias_table, col_hot, precision=lax.Precision.HIGHEST)
    bias_win = jnp.einsum("rke,heqw->rqhkw", row_hot, col_table, precision=lax.Precision.HIGHEST)
    inv_scale = HEAD_DIM ** (-0.5)
    scores_win = (
        jnp.einsum("rqhd,rkwhd->rqhkw", queries, key_win, preferred_element_type=jnp.float32)
        * inv_scale
        + bias_win
    )
    scores_win = jnp.where(col_in[None, :, None, None, :], scores_win, NEG_BIG)
    scores_win = scores_win.reshape(grid_rows, GRID_W, head_dev, WIN_H * GRID_W)
    scores_ctx = (
        jnp.einsum("rqhd,chd->rqhc", queries, ctx_key3, preferred_element_type=jnp.float32)
        * inv_scale
    )
    row_max = jnp.maximum(jnp.max(scores_win, axis=-1), jnp.max(scores_ctx, axis=-1))
    exp_win = jnp.exp(scores_win - row_max[..., None])
    exp_ctx = jnp.exp(scores_ctx - row_max[..., None])
    row_total = jnp.sum(exp_win, axis=-1) + jnp.sum(exp_ctx, axis=-1)
    probs_win = (exp_win / row_total[..., None]).astype(jnp.bfloat16)
    probs_win = probs_win.reshape(grid_rows, GRID_W, head_dev, WIN_H, GRID_W)
    probs_ctx = (exp_ctx / row_total[..., None]).astype(jnp.bfloat16)
    attended = jnp.einsum(
        "rqhkw,rkwhd->rqhd", probs_win, val_win, preferred_element_type=jnp.float32
    )
    attended = attended + jnp.einsum(
        "rqhc,chd->rqhd", probs_ctx, ctx_val3, preferred_element_type=jnp.float32
    )
    attended = attended.astype(jnp.bfloat16).reshape(grid_rows * GRID_W, head_cols)
    branch = lax.psum_scatter(
        jnp.dot(attended, w_out, preferred_element_type=jnp.float32).astype(jnp.bfloat16),
        "tp",
        scatter_dimension=0,
        tiled=True,
    ).astype(jnp.float32)
    return (latent.astype(jnp.float32) + mod_vecs[4] * branch).astype(jnp.bfloat16)


def solution(mesh):
    placed = (
        P(("sp", "tp"), None),
        P("sp", None),
        P(),
        P(),
        P(),
        P("sp", "tp"),
        P("sp", "tp"),
        P("sp", "tp"),
        P(None, "tp"),
        P(None, "tp"),
        P(None, "tp"),
        P("tp", None),
        P(),
    )
    return jax.shard_map(
        on_device, mesh=mesh, in_specs=placed, out_specs=P(("sp", "tp"), None), check_vma=False
    )
```

profile of v0, /device:TPU:0, one launch (start us, length us, event | category | flops | bytes accessed | tf_op | source)
XLA Modules:
  0.0 193.7 jit_solution(12751256618278326930)
XLA Ops:
  6.6 0.8 fusion.61
  7.4 0.2 copy-done
  7.5 0.1 fusion.69
  7.7 1.1 fusion.70
  8.8 1.1 fusion.63
  9.9 42.3 %psum.7 = f32[5,2048]{1,0:T(8,128)S(1)} all-reduce(f32[5,2048]{1,0:T(8,128)S(1)} %maximum_dynamic-update-slice_fusion), channel_id=1, replica_groups=mesh['sp'=16,'tp'=2] {'sp','tp'}, use_global_device_ids=true, to_apply=%region_0.1 | all-reduce | flops 10240 | bytes 81920 | tf_op jit(solution)/shard_map/psum | solution.py:84
  52.2 1.2 fusion.35
  53.5 2.1 %fusion.39 = bf16[128,2048]{1,0:T(8,128)(2,1)} fusion(bf16[128,2048]{1,0:T(8,128)(2,1)} %param.13, f32[2048]{0:T(1024)S(1)} %bitcast.155, f32[2048]{0:T(1024)S(1)} %bitcast.156, f32[2048]{0:T(1024)} %param.17, f32[128]{0:T(128)S(1)} %add_rsqrt_fusion.1), kind=kLoop, calls=%fused_computation.46 | loop fusion | flops 1572864 | bytes 1073664 | tf_op jit(solution)/shard_map/convert_element_type | solution.py:37
  55.7 1.3 fusion.41
  57.0 3.2 %fusion.33 = bf16[1,64,1024]{2,1,0:T(8,128)(2,1)S(1)} fusion(bf16[2048,1024]{1,0:T(8,128)(2,1)} %param.22, bf16[64,2048]{1,0:T(8,128)(2,1)} %param.14, f32[2048]{0:T(1024)S(1)} %bitcast.150, f32[2048]{0:T(1024)S(1)} %bitcast.152, f32[2048]{0:T(1024)} %param.17, f32[64]{0:T(128)S(1)} %add_rsqrt_fusion), kind=kOutput, calls=%fused_computation.40 | convolution fusion | flops 269287424 | bytes 4612352 | tf_op jit(solution)/shard_map/dot_general | solution.py:43
  60.2 0.9 fusion.34
  61.1 0.7 pad_maximum_fusion.2
  62.1 1.4 fusion.51
  63.5 5.6 %fusion.12 = f32[8,32,32,8,8]{2,4,3,1,0:T(8,128)} fusion(f32[8,15,32,32]{3,1,2,0:T(8,128)S(1)} %fusion.51, s32[8,8]{1,0:T(8,128)S(1)} %subtract_add_fusion), kind=kOutput, calls=%fused_computation.21 | convolution fusion | flops 94372800 | bytes 2588928 | tf_op jit(solution)/shard_map/rke,heqw->rqhkw/dot_general | solution.py:132
  69.2 9.3 %copy.59 = f32[8,32,32,8,8]{1,2,4,0,3:T(8,128)} copy(f32[8,32,32,8,8]{2,4,3,1,0:T(8,128)} %fusion.12) | data formatting | bytes 4194304 | tf_op jit(solution)/shard_map/rke,heqw->rqhkw/dot_general | solution.py:132
  78.5 3.9 %convolution_convert_fusion.2 = bf16[256,1024]{1,0:T(8,128)(2,1)S(1)} fusion(bf16[256,2048]{1,0:T(8,128)(2,1)} %all-gather.3.cloned.1.call-done, bf16[2048,1024]{1,0:T(8,128)(2,1)} %param.23), kind=kOutput, calls=%fused_computation.35 | convolution fusion | flops 1074003968 | bytes 5767168 | tf_op jit(solution)/shard_map/dot_general | solution.py:43
  82.4 0.1 copy-done.10
  82.6 1.3 convolution_convert_fusion.3
  83.8 0.1 fusion.46
  83.9 4.2 %collective-permute-start = (bf16[2,4,32,1024]{3,2,0,1:T(8,128)(2,1)S(1)}, bf16[2,4,32,1024]{3,2,0,1:T(8,128)(2,1)S(1)}, u32[]{:S(2)}, u32[]{:S(2)}) collective-permute-start(bf16[2,4,32,1024]{3,2,0,1:T(8,128)(2,1)S(1)} %get-tuple-element.9), channel_id=1, source_target_pairs={{0,2},{2,4},{4,6},{6,8},{8,10},{10,12},{12,14},{14,16},{16,18},{18... | collective-permute-start | bytes 1572872 | tf_op jit(solution)/shard_map/ppermute | solution.py:23
  88.2 1.3 collective-permute-start.1
  89.5 1.3 fusion.32
  90.8 0.1 copy.82
  90.9 0.1 copy.61
  91.0 25.2 %collective-permute-done = bf16[2,4,32,1024]{3,2,0,1:T(8,128)(2,1)S(1)} collective-permute-done((bf16[2,4,32,1024]{3,2,0,1:T(8,128)(2,1)S(1)}, bf16[2,4,32,1024]{3,2,0,1:T(8,128)(2,1)S(1)}, u32[]{:S(2)}, u32[]{:S(2)}) %collective-permute-start) | collective-permute-done | bytes 524320 | tf_op jit(solution)/shard_map/ppermute | solution.py:23
  116.2 1.9 collective-permute-done.1
  118.1 0.3 pad_maximum_fusion
  118.4 4.9 %gather_fusion = bf16[8,2,8,32,1024]{4,3,1,2,0:T(8,128)(2,1)} fusion(bf16[2,16,32,1024]{3,2,0,1:T(8,128)(2,1)S(1)} %pad_maximum_fusion, s32[8]{0:T(128)S(1)} %shift-left_bitcast_fusion), kind=kCustom, calls=%fused_computation | custom fusion | bytes 16777344 | tf_op jit(solution)/shard_map/vmap()/gather | solution.py:109
  123.3 4.0 %fusion.66 = (bf16[8,1,8,32,1024]{4,3,1,2,0:T(8,128)(2,1)S(1)}, bf16[8,1,8,32,1024]{4,3,1,2,0:T(8,128)(2,1)S(1)}) fusion(bf16[8,2,8,32,1024]{4,3,1,2,0:T(8,128)(2,1)} %gather_fusion), kind=kLoop, calls=%fused_computation.99 | loop fusion | bytes 16777216 | tf_op jit(solution)/shard_map/slice | solution.py:113
  127.3 1.1 copy.81
  128.4 3.3 %copy.80 = bf16[256,8,8,128]{3,2,1,0:T(8,128)(2,1)} copy(bf16[256,8,8,128]{3,1,2,0:T(8,128)(2,1)S(1)} %bitcast.137) | data formatting | bytes 8388608
  131.7 1.2 slice-done.1
  132.9 4.3 %fusion.68 = (f32[8,32,8]{1,2,0:T(8,128)S(1)}, f32[8,32,8,8,32]{1,4,3,2,0:T(8,128)}) fusion(f32[8,32,32,8,8]{1,2,4,0,3:T(8,128)S(1)} %bitcast.133, bf16[8,32,8,128,1]{3,2,1,0,4:T(8,128)(2,1)S(1)} %bitcast_bitcast_fusion, bf16[8,8,32,8,128]{4,3,2,1,0:T(8,128)(2,1)S(1)} %bitcast.136, pred[32,32]{0,1:T(8,128)(4,1)S(1)} %fusion.57), kind=kOutput, calls=%fused_computation.101 | convolution fusion | flops 136312832 | bytes 8922112 | tf_op jit(solution)/shard_map/rqhd,rkwhd->rqhkw/dot_general | solution.py:135
  137.2 19.0 %all-gather.5.cloned.1.call-done = bf16[2,1024,1024]{2,1,0:T(8,128)(2,1)} async-done(((bf16[2,64,1024]{2,1,0:T(8,128)(2,1)}), bf16[2,1024,1024]{2,1,0:T(8,128)(2,1)}) %all-gather.5.cloned.1.call-update) | async-done | bytes 4194320 | tf_op jit(solution)/shard_map/all_gather | solution.py:87
  156.2 3.2 %slice_bitcast_fusion = (bf16[128,8,8,128]{3,1,2,0:T(8,128)(2,1)S(1)}, bf16[128,8,8,128]{3,1,2,0:T(8,128)(2,1)S(1)}) fusion(bf16[2,1024,1024]{2,1,0:T(8,128)(2,1)} %all-gather.5.cloned.1.call-done), kind=kLoop, calls=%fused_computation.18 | loop fusion | bytes 8388608
  159.4 0.6 copy.83
  160.0 1.3 fusion.16
  161.3 0.7 bitcast_reduce_fusion
  162.0 1.9 fusion.3
  163.9 1.0 slice-done.3
  164.9 2.0 %fusion.2 = f32[8,32,8]{1,2,0:T(8,128)S(1)} fusion(f32[8,32,8,8,32]{1,4,3,2,0:T(8,128)S(1)} %bitcast.135, f32[8,32,8]{1,2,0:T(8,128)S(1)} %copy_maximum_fusion), kind=kLoop, calls=%fused_computation.9 | loop fusion | flops 1046528 | bytes 2113536 | tf_op jit(solution)/shard_map/reduce_sum | solution.py:148
  167.0 0.6 copy.84
  167.6 3.3 %fusion.21 = f32[8,32,8,128]{3,1,2,0:T(8,128)S(1)} fusion(bf16[1024,8,128]{2,1,0:T(8,128)(2,1)S(1)} %bitcast.143, f32[8,32,8]{1,0,2:T(8,128)S(1)} %copy.67, f32[8,32,8]{1,0,2:T(8,128)S(1)} %copy.63, f32[8,1024,256]{1,2,0:S(1)} %fusion.16), kind=kOutput, calls=%fused_computation.31 | convolution fusion | flops 545259520 | bytes 11550720 | tf_op jit(solution)/shard_map/rqhc,chd->rqhd/dot_general | solution.py:155
  170.9 2.3 %fusion.29 = bf16[8,32,8,128]{3,1,2,0:T(8,128)(2,1)S(1)} fusion(f32[8,32,8,128]{3,1,2,0:T(8,128)S(1)} %fusion.21, f32[8,32,8,8,32]{1,4,3,2,0:T(8,128)S(1)} %bitcast.135, f32[8,32,8]{1,2,0:T(8,128)S(1)} %copy_add_fusion, f32[8,32,8]{1,2,0:T(8,128)S(1)} %copy_maximum_fusion, bf16[8,8,32,8,128]{4,3,2,1,0:T(8,128)(2,1)S(1)} %bitcast.142), kind=kOutput, calls=%fused_computation.33 | convolution fusion | flops 136314880 | bytes 7880704 | tf_op jit(solution)/shard_map/rqhkw,rkwhd->rqhd/dot_general | solution.py:152
  173.2 0.2 copy.70
  173.5 4.5 %convolution_convert_fusion = bf16[256,2048]{1,0:T(8,128)(2,1)} fusion(bf16[1024,2048]{1,0:T(8,128)(2,1)} %param.24, bf16[32,8,8,128]{3,2,1,0:T(8,128)(2,1)S(1)} %bitcast.149), kind=kOutput, calls=%fused_computation.17 | convolution fusion | flops 1074266112 | bytes 5767168 | tf_op jit(solution)/shard_map/dot_general | solution.py:160
  178.0 7.1 %reduce-scatter.2.cloned.1.call-done = bf16[128,2048]{1,0:T(8,128)(2,1)} async-done(((bf16[256,2048]{1,0:T(8,128)(2,1)}), bf16[128,2048]{1,0:T(8,128)(2,1)}) %reduce-scatter.2.cloned.1.call-update) | async-done | bytes 524304 | tf_op jit(solution)/shard_map/reduce_scatter | solution.py:159
  185.1 2.0 %fusion.40 = bf16[128,2048]{1,0:T(8,128)(2,1)} fusion(bf16[128,2048]{1,0:T(8,128)(2,1)S(1)} %copy-done.2, bf16[128,2048]{1,0:T(8,128)(2,1)} %reduce-scatter.2.cloned.1.call-done, f32[2048]{0:T(1024)S(1)} %bitcast.154), kind=kLoop, calls=%fused_computation.47 | loop fusion | flops 1310720 | bytes 1581056 | tf_op jit(solution)/shard_map/convert_element_type | solution.py:165
  (52 shorter events, 0.5 us)
Async XLA Ops:
  6.5 1.0 copy-start
  6.5 53.7 %copy-start.7 = (f32[2048]{0:T(1024)S(1)}, f32[2048]{0:T(1024)}, u32[]{:S(2)}) copy-start(f32[2048]{0:T(1024)} %param.17) | copy-start | bytes 24580
  6.5 53.7 %copy-start.6 = (bf16[64,2048]{1,0:T(8,128)(2,1)S(1)}, bf16[64,2048]{1,0:T(8,128)(2,1)}, u32[]{:S(2)}) copy-start(bf16[64,2048]{1,0:T(8,128)(2,1)} %param.14) | copy-start | bytes 786436
  6.5 72.0 %all-gather.3.cloned.1.call-start = ((), (), s32[]{:S(2)}) async-start(), calls=%async_computation.1 | async-start | bytes 1572864 | tf_op jit(solution)/shard_map/all_gather | solution.py:86
  55.6 100.6 %all-gather.5.cloned.1.call-start = ((), (), s32[]{:S(2)}) async-start(), calls=%async_computation.2 | async-start | bytes 4456448 | tf_op jit(solution)/shard_map/all_gather | solution.py:87
  55.7 4.6 %copy-start.3 = (bf16[2048,1024]{1,0:T(8,128)(2,1)S(1)}, bf16[2048,1024]{1,0:T(8,128)(2,1)}, u32[]{:S(2)}) copy-start(bf16[2048,1024]{1,0:T(8,128)(2,1)} %param.23) | copy-start | bytes 12582916
  56.9 5.0 %copy-start.8 = (f32[16,15,31]{2,0,1:T(8,128)S(1)}, f32[16,15,31]{2,0,1:T(8,128)}, u32[]{:S(2)}) copy-start(f32[16,15,31]{2,0,1:T(8,128)} %param.25) | copy-start | bytes 89284
  61.9 123.2 %reduce-scatter.2.cloned.1.call-start = ((), (), s32[]{:S(2)}) async-start(), calls=%async_computation.3 | async-start | bytes 1572864 | tf_op jit(solution)/shard_map/reduce_scatter | solution.py:159
  78.5 3.9 %copy-start.4 = (bf16[2048,1024]{1,0:T(8,128)(2,1)S(1)}, bf16[2048,1024]{1,0:T(8,128)(2,1)}, u32[]{:S(2)}) copy-start(bf16[2048,1024]{1,0:T(8,128)(2,1)} %param.22) | copy-start | bytes 12582916
  78.5 4.0 %copy-start.10 = (bf16[256,2048]{1,0:T(8,128)(2,1)S(1)}, bf16[256,2048]{1,0:T(8,128)(2,1)}, u32[]{:S(2)}) copy-start(bf16[256,2048]{1,0:T(8,128)(2,1)} %all-gather.3.cloned.1.call-done) | copy-start | bytes 3145732
  82.6 6.9 %copy-start.9 = (bf16[2048,1024]{1,0:T(8,128)(2,1)S(1)}, bf16[2048,1024]{1,0:T(8,128)(2,1)}, u32[]{:S(2)}) copy-start(bf16[2048,1024]{1,0:T(8,128)(2,1)} %param.21) | copy-start | bytes 12582916
  83.9 32.3 %collective-permute-start = (bf16[2,4,32,1024]{3,2,0,1:T(8,128)(2,1)S(1)}, bf16[2,4,32,1024]{3,2,0,1:T(8,128)(2,1)S(1)}, u32[]{:S(2)}, u32[]{:S(2)}) collective-permute-start(bf16[2,4,32,1024]{3,2,0,1:T(8,128)(2,1)S(1)} %get-tuple-element.9), channel_id=1, source_target_pairs={{0,2},{2,4},{4,6},{6,8},{8,10},{10,12},{12,14},{14,16},{16,18},{18... | collective-permute-start | bytes 1572872 | tf_op jit(solution)/shard_map/ppermute | solution.py:23
  88.2 30.0 %collective-permute-start.1 = (bf16[2,4,32,1024]{3,2,0,1:T(8,128)(2,1)S(1)}, bf16[2,4,32,1024]{3,2,0,1:T(8,128)(2,1)S(1)}, u32[]{:S(2)}, u32[]{:S(2)}) collective-permute-start(bf16[2,4,32,1024]{3,2,0,1:T(8,128)(2,1)S(1)} %get-tuple-element.10), channel_id=1, source_target_pairs={{2,0},{4,2},{6,4},{8,6},{10,8},{12,10},{14,12},{16,14},{18,16},{20... | collective-permute-start | bytes 1572872 | tf_op jit(solution)/shard_map/ppermute | solution.py:25
  127.3 4.5 %slice-start = ((s8[8388608]{0:T(1024)(128)(4,1)}), s8[4194304]{0:T(1024)(128)(4,1)S(1)}, s32[]{:S(2)}) async-start(s8[8388608]{0:T(1024)(128)(4,1)} %bitcast.132), calls=%async_computation.4 | async-start | bytes 8388608
  128.4 4.5 %slice-start.1 = ((s8[8388608]{0:T(1024)(128)(4,1)}), s8[4194304]{0:T(1024)(128)(4,1)S(1)}, s32[]{:S(2)}) async-start(s8[8388608]{0:T(1024)(128)(4,1)} %bitcast.132), calls=%async_computation.5 | async-start | bytes 8388608
  161.3 2.6 %slice-start.2 = ((s8[8388608]{0:T(1024)(128)(4,1)}), s8[4194304]{0:T(1024)(128)(4,1)S(1)}, s32[]{:S(2)}) async-start(s8[8388608]{0:T(1024)(128)(4,1)} %bitcast.134), calls=%async_computation.6 | async-start | bytes 8388608
  162.0 2.9 %slice-start.3 = ((s8[8388608]{0:T(1024)(128)(4,1)}), s8[4194304]{0:T(1024)(128)(4,1)S(1)}, s32[]{:S(2)}) async-start(s8[8388608]{0:T(1024)(128)(4,1)} %bitcast.134), calls=%async_computation.7 | async-start | bytes 8388608
  167.6 3.3 %copy-start.5 = (bf16[256,8,8,128]{3,2,1,0:T(8,128)(2,1)S(1)}, bf16[256,8,8,128]{3,2,1,0:T(8,128)(2,1)}, u32[]{:S(2)}) copy-start(bf16[256,8,8,128]{3,2,1,0:T(8,128)(2,1)} %copy.80) | copy-start | bytes 12582916
  173.5 11.7 %copy-start.2 = (bf16[128,2048]{1,0:T(8,128)(2,1)S(1)}, bf16[128,2048]{1,0:T(8,128)(2,1)}, u32[]{:S(2)}) copy-start(bf16[128,2048]{1,0:T(8,128)(2,1)} %param.13) | copy-start | bytes 1572868
  173.5 13.6 %copy-start.1 = (bf16[128,1024]{1,0:T(8,128)(2,1)S(1)}, bf16[128,1024]{1,0:T(8,128)(2,1)}, u32[]{:S(2)}) copy-start(bf16[128,1024]{1,0:T(8,128)(2,1)} %param.18) | copy-start | bytes 786436
Sparse Core Ops, SparseCore 0:
  55.7 8.8 all-gather.2
  67.3 88.8 all-gather.4
  178.1 6.9 reduce-scatter.1
where the time goes:
time: 194 us
  waiting for transfers between devices  53.3 us (27%)
  blocking collectives  42.3 us (22%)
  matrix products  35.6 us (18%)
  local copies, waits for them, and re-layouts  30 us (15%)
  between operations  13.6 us (7%)
  other arithmetic  13.3 us (7%)
  starting transfers between devices  5.61 us (3%)
    psum x1, blocking collectives, on_device(): mod_vecs = lax.psum(placed, ('sp', 'tp'))  42.3 us
    ppermute x1, waiting for transfers between devices, padded_2(): lax.ppermute(tail, axis, [(i, (i + 1) % count) for i in range(ends)])  25.2 us
    all_gather x1, waiting for transfers between devices, on_device(): lax.all_gather(project(rms_mod(context, norm_gain, mod_vecs[1], mod_vecs[...  19 us
    unnamed x36, local copies, waits for them, and re-layouts  11.5 us
    dot_general x5, matrix products, project(): jnp.dot(block, weight, preferred_element_type=jnp.float32)  10.6 us
    dot_general x1, local copies, waits for them, and re-layouts, on_device(): jnp.einsum('rke,heqw->rqhkw', row_hot, col_table, precision=lax.Precision...  9.27 us
    reduce_scatter x1, waiting for transfers between devices, on_device(): lax.psum_scatter(jnp.dot(attended, w_out, preferred_element_type=jnp.floa...  7.12 us
    dot_general x1, matrix products, on_device(): jnp.einsum('rke,heqw->rqhkw', row_hot, col_table, precision=lax.Precision...  5.61 us
  transfers between devices with their start and end apart: 5, of which 4 were waited for; matrix products, arithmetic and copies ran while one was open for 24% of the time, Pallas kernels for 0%

commit v1 on v0

--- a/solution.py
+++ b/solution.py
@@ -81,7 +81,13 @@
     placed = lax.dynamic_update_slice_in_dim(
         jnp.zeros((5, model_width), jnp.float32), partial_value, lax.axis_index("tp") * col_part, 1
     )
-    mod_vecs = lax.psum(placed, ("sp", "tp"))
+
+    def wall_settle(piece_in, shard_axis, mesh_ax="sp"):
+        for hop_no in (shard_axis, mesh_ax):
+            piece_in = lax.psum(piece_in, hop_no)
+        return piece_in
+
+    mod_vecs = wall_settle(placed, "tp")
     normed = rms_mod(latent, norm_gain, mod_vecs[0], mod_vecs[2])
     projected = project(lax.all_gather(normed, "tp", axis=0, tiled=True), (w_query, w_key, w_value))
     ctx_kv = lax.all_gather(

time: 194 us -> 222 us (1.14)
  blocking collectives: 42.3 us -> 82.3 us
  waiting for transfers between devices: 53.3 us -> 43.5 us
  starting transfers between devices: 5.61 us -> 2.7 us
    psum x1 -> x2, blocking collectives: 42.3 us -> 82.3 us  [wall_settle(): piece_in = lax.psum(piece_in, hop_no)]
    ppermute x1, waiting for transfers between devices: 25.2 us -> 16.8 us  [padded_2(): lax.ppermute(tail, axis, [(i, (i + 1) % count) for i in range(ends)])]
    ppermute x1, starting transfers between devices: 4.23 us -> 1.32 us  [padded_2(): lax.ppermute(tail, axis, [(i, (i + 1) % count) for i in range(ends)])]
  transfers between devices with their start and end apart: 5 -> 5, of which waited for: 4 -> 3; matrix products, arithmetic and copies ran while one was open for 24% -> 22% of each run, Pallas kernels for 0% -> 0%
where the time goes in v1:
time: 222 us; the launch traced here: 221 us
  blocking collectives  82.3 us (37%)
  waiting for transfers between devices  43.5 us (20%)
  matrix products  36.1 us (16%)
  local copies, waits for them, and re-layouts  30 us (14%)
  between operations  13.6 us (6%)
  other arithmetic  13.3 us (6%)
  starting transfers between devices  2.7 us (1%)
    psum x2, blocking collectives, wall_settle(): piece_in = lax.psum(piece_in, hop_no)  82.3 us
    all_gather x1, waiting for transfers between devices, on_device(): lax.all_gather(project(rms_mod(context, norm_gain, mod_vecs[1], mod_vecs[...  19.5 us
    ppermute x1, waiting for transfers between devices, padded_2(): lax.ppermute(tail, axis, [(i, (i + 1) % count) for i in range(ends)])  16.8 us
    unnamed x36, local copies, waits for them, and re-layouts  11.5 us
    dot_general x5, matrix products, project(): jnp.dot(block, weight, preferred_element_type=jnp.float32)  11 us
    dot_general x1, local copies, waits for them, and re-layouts, on_device(): jnp.einsum('rke,heqw->rqhkw', row_hot, col_table, precision=lax.Precision...  9.26 us
    reduce_scatter x1, waiting for transfers between devices, on_device(): lax.psum_scatter(jnp.dot(attended, w_out, preferred_element_type=jnp.floa...  7.12 us
    dot_general x1, matrix products, on_device(): jnp.einsum('rke,heqw->rqhkw', row_hot, col_table, precision=lax.Precision...  5.63 us
  transfers between devices with their start and end apart: 5, of which 3 were waited for; matrix products, arithmetic and copies ran while one was open for 22% of the time, Pallas kernels for 0%

profile of v1, /device:TPU:0, one launch (start us, length us, event | category | flops | bytes accessed | tf_op | source)
XLA Modules:
  0.0 221.4 jit_solution(14409335116672816486)
XLA Ops:
  6.6 0.8 fusion.61
  7.4 0.2 copy-done
  7.5 0.1 fusion.69
  7.7 1.1 fusion.70
  8.8 1.1 fusion.63
  9.9 3.9 %psum.14 = f32[5,2048]{1,0:T(8,128)S(1)} all-reduce(f32[5,2048]{1,0:T(8,128)S(1)} %maximum_dynamic-update-slice_fusion), channel_id=1, replica_groups=mesh['sp'=16,'tp'=2] {'tp'}, use_global_device_ids=true, to_apply=%region_0.1 | all-reduce | flops 10240 | bytes 81920 | tf_op jit(solution)/shard_map/psum | solution.py:87
  13.8 78.3 %psum.15 = f32[5,2048]{1,0:T(8,128)S(1)} all-reduce(f32[5,2048]{1,0:T(8,128)S(1)} %psum.14), channel_id=1, replica_groups=mesh['sp'=16,'tp'=2] {'sp'}, use_global_device_ids=true, to_apply=%region_1.2 | all-reduce | flops 10240 | bytes 81920 | tf_op jit(solution)/shard_map/psum | solution.py:87
  92.2 1.2 fusion.35
  93.4 2.1 fusion.39
  95.6 1.3 fusion.41
  96.9 3.6 %fusion.33 = bf16[1,64,1024]{2,1,0:T(8,128)(2,1)S(1)} fusion(bf16[2048,1024]{1,0:T(8,128)(2,1)} %param.22, bf16[64,2048]{1,0:T(8,128)(2,1)} %param.14, f32[2048]{0:T(1024)S(1)} %bitcast.150, f32[2048]{0:T(1024)S(1)} %bitcast.152, f32[2048]{0:T(1024)} %param.17, f32[64]{0:T(128)S(1)} %add_rsqrt_fusion), kind=kOutput, calls=%fused_computation.40 | convolution fusion | flops 269287424 | bytes 4612352 | tf_op jit(solution)/shard_map/dot_general | solution.py:43
  100.6 0.9 fusion.34
  101.5 0.7 pad_maximum_fusion.2
  102.4 1.4 fusion.51
  103.9 5.6 %fusion.12 = f32[8,32,32,8,8]{2,4,3,1,0:T(8,128)} fusion(f32[8,15,32,32]{3,1,2,0:T(8,128)S(1)} %fusion.51, s32[8,8]{1,0:T(8,128)S(1)} %subtract_add_fusion), kind=kOutput, calls=%fused_computation.21 | convolution fusion | flops 94372800 | bytes 2588928 | tf_op jit(solution)/shard_map/rke,heqw->rqhkw/dot_general | solution.py:138
  109.5 9.3 %copy.59 = f32[8,32,32,8,8]{1,2,4,0,3:T(8,128)} copy(f32[8,32,32,8,8]{2,4,3,1,0:T(8,128)} %fusion.12) | data formatting | bytes 4194304 | tf_op jit(solution)/shard_map/rke,heqw->rqhkw/dot_general | solution.py:138
  118.9 3.9 %convolution_convert_fusion.2 = bf16[256,1024]{1,0:T(8,128)(2,1)S(1)} fusion(bf16[256,2048]{1,0:T(8,128)(2,1)} %all-gather.3.cloned.1.call-done, bf16[2048,1024]{1,0:T(8,128)(2,1)} %param.23), kind=kOutput, calls=%fused_computation.35 | convolution fusion | flops 1074003968 | bytes 5767168 | tf_op jit(solution)/shard_map/dot_general | solution.py:43
  122.8 0.1 copy-done.10
  122.9 1.3 convolution_convert_fusion.3
  124.2 0.1 fusion.46
  124.3 1.3 collective-permute-start
  125.6 1.3 collective-permute-start.1
  126.9 1.3 fusion.32
  128.2 0.1 copy.82
  128.3 0.1 copy.61
  128.4 16.8 %collective-permute-done = bf16[2,4,32,1024]{3,2,0,1:T(8,128)(2,1)S(1)} collective-permute-done((bf16[2,4,32,1024]{3,2,0,1:T(8,128)(2,1)S(1)}, bf16[2,4,32,1024]{3,2,0,1:T(8,128)(2,1)S(1)}, u32[]{:S(2)}, u32[]{:S(2)}) %collective-permute-start) | collective-permute-done | bytes 524320 | tf_op jit(solution)/shard_map/ppermute | solution.py:23
  145.3 0.3 pad_maximum_fusion
  145.5 4.9 %gather_fusion = bf16[8,2,8,32,1024]{4,3,1,2,0:T(8,128)(2,1)} fusion(bf16[2,16,32,1024]{3,2,0,1:T(8,128)(2,1)S(1)} %pad_maximum_fusion, s32[8]{0:T(128)S(1)} %shift-left_bitcast_fusion), kind=kCustom, calls=%fused_computation | custom fusion | bytes 16777344 | tf_op jit(solution)/shard_map/vmap()/gather | solution.py:115
  150.4 4.0 %fusion.66 = (bf16[8,1,8,32,1024]{4,3,1,2,0:T(8,128)(2,1)S(1)}, bf16[8,1,8,32,1024]{4,3,1,2,0:T(8,128)(2,1)S(1)}) fusion(bf16[8,2,8,32,1024]{4,3,1,2,0:T(8,128)(2,1)} %gather_fusion), kind=kLoop, calls=%fused_computation.99 | loop fusion | bytes 16777216 | tf_op jit(solution)/shard_map/slice | solution.py:119
  154.4 1.1 copy.81
  155.5 3.3 %copy.80 = bf16[256,8,8,128]{3,2,1,0:T(8,128)(2,1)} copy(bf16[256,8,8,128]{3,1,2,0:T(8,128)(2,1)S(1)} %bitcast.137) | data formatting | bytes 8388608
  158.8 1.3 slice-done.1
  160.1 4.3 %fusion.68 = (f32[8,32,8]{1,2,0:T(8,128)S(1)}, f32[8,32,8,8,32]{1,4,3,2,0:T(8,128)}) fusion(f32[8,32,32,8,8]{1,2,4,0,3:T(8,128)S(1)} %bitcast.133, bf16[8,32,8,128,1]{3,2,1,0,4:T(8,128)(2,1)S(1)} %bitcast_bitcast_fusion, bf16[8,8,32,8,128]{4,3,2,1,0:T(8,128)(2,1)S(1)} %bitcast.136, pred[32,32]{0,1:T(8,128)(4,1)S(1)} %fusion.57), kind=kOutput, calls=%fused_computation.101 | convolution fusion | flops 136312832 | bytes 8922112 | tf_op jit(solution)/shard_map/rqhd,rkwhd->rqhkw/dot_general | solution.py:141
  164.4 19.5 %all-gather.5.cloned.1.call-done = bf16[2,1024,1024]{2,1,0:T(8,128)(2,1)} async-done(((bf16[2,64,1024]{2,1,0:T(8,128)(2,1)}), bf16[2,1024,1024]{2,1,0:T(8,128)(2,1)}) %all-gather.5.cloned.1.call-update) | async-done | bytes 4194320 | tf_op jit(solution)/shard_map/all_gather | solution.py:93
  184.0 3.2 %slice_bitcast_fusion = (bf16[128,8,8,128]{3,1,2,0:T(8,128)(2,1)S(1)}, bf16[128,8,8,128]{3,1,2,0:T(8,128)(2,1)S(1)}) fusion(bf16[2,1024,1024]{2,1,0:T(8,128)(2,1)} %all-gather.5.cloned.1.call-done), kind=kLoop, calls=%fused_computation.18 | loop fusion | bytes 8388608
  187.1 0.6 copy.83
  187.8 1.3 fusion.16
  189.1 0.7 bitcast_reduce_fusion
  189.8 1.9 fusion.3
  191.7 1.0 slice-done.3
  192.7 2.0 fusion.2
  194.8 0.6 copy.84
  195.4 3.3 %fusion.21 = f32[8,32,8,128]{3,1,2,0:T(8,128)S(1)} fusion(bf16[1024,8,128]{2,1,0:T(8,128)(2,1)S(1)} %bitcast.143, f32[8,32,8]{1,0,2:T(8,128)S(1)} %copy.67, f32[8,32,8]{1,0,2:T(8,128)S(1)} %copy.63, f32[8,1024,256]{1,2,0:S(1)} %fusion.16), kind=kOutput, calls=%fused_computation.31 | convolution fusion | flops 545259520 | bytes 11550720 | tf_op jit(solution)/shard_map/rqhc,chd->rqhd/dot_general | solution.py:161
  198.7 2.3 %fusion.29 = bf16[8,32,8,128]{3,1,2,0:T(8,128)(2,1)S(1)} fusion(f32[8,32,8,128]{3,1,2,0:T(8,128)S(1)} %fusion.21, f32[8,32,8,8,32]{1,4,3,2,0:T(8,128)S(1)} %bitcast.135, f32[8,32,8]{1,2,0:T(8,128)S(1)} %copy_add_fusion, f32[8,32,8]{1,2,0:T(8,128)S(1)} %copy_maximum_fusion, bf16[8,8,32,8,128]{4,3,2,1,0:T(8,128)(2,1)S(1)} %bitcast.142), kind=kOutput, calls=%fused_computation.33 | convolution fusion | flops 136314880 | bytes 7880704 | tf_op jit(solution)/shard_map/rqhkw,rkwhd->rqhd/dot_general | solution.py:158
  201.0 0.2 copy.70
  201.3 4.5 %convolution_convert_fusion = bf16[256,2048]{1,0:T(8,128)(2,1)} fusion(bf16[1024,2048]{1,0:T(8,128)(2,1)} %param.24, bf16[32,8,8,128]{3,2,1,0:T(8,128)(2,1)S(1)} %bitcast.149), kind=kOutput, calls=%fused_computation.17 | convolution fusion | flops 1074266112 | bytes 5767168 | tf_op jit(solution)/shard_map/dot_general | solution.py:166
  205.8 7.1 %reduce-scatter.2.cloned.1.call-done = bf16[128,2048]{1,0:T(8,128)(2,1)} async-done(((bf16[256,2048]{1,0:T(8,128)(2,1)}), bf16[128,2048]{1,0:T(8,128)(2,1)}) %reduce-scatter.2.cloned.1.call-update) | async-done | bytes 524304 | tf_op jit(solution)/shard_map/reduce_scatter | solution.py:165
  212.9 2.0 fusion.40
  (53 shorter events, 0.5 us)
Async XLA Ops:
  6.5 1.0 copy-start
  6.5 94.0 %copy-start.7 = (f32[2048]{0:T(1024)S(1)}, f32[2048]{0:T(1024)}, u32[]{:S(2)}) copy-start(f32[2048]{0:T(1024)} %param.17) | copy-start | bytes 24580
  6.5 94.0 %copy-start.6 = (bf16[64,2048]{1,0:T(8,128)(2,1)S(1)}, bf16[64,2048]{1,0:T(8,128)(2,1)}, u32[]{:S(2)}) copy-start(bf16[64,2048]{1,0:T(8,128)(2,1)} %param.14) | copy-start | bytes 786436
  6.5 112.3 %all-gather.3.cloned.1.call-start = ((), (), s32[]{:S(2)}) async-start(), calls=%async_computation.1 | async-start | bytes 1572864 | tf_op jit(solution)/shard_map/all_gather | solution.py:92
  95.6 88.4 %all-gather.5.cloned.1.call-start = ((), (), s32[]{:S(2)}) async-start(), calls=%async_computation.2 | async-start | bytes 4456448 | tf_op jit(solution)/shard_map/all_gather | solution.py:93
  95.6 4.9 %copy-start.3 = (bf16[2048,1024]{1,0:T(8,128)(2,1)S(1)}, bf16[2048,1024]{1,0:T(8,128)(2,1)}, u32[]{:S(2)}) copy-start(bf16[2048,1024]{1,0:T(8,128)(2,1)} %param.23) | copy-start | bytes 12582916
  96.9 5.4 %copy-start.8 = (f32[16,15,31]{2,0,1:T(8,128)S(1)}, f32[16,15,31]{2,0,1:T(8,128)}, u32[]{:S(2)}) copy-start(f32[16,15,31]{2,0,1:T(8,128)} %param.25) | copy-start | bytes 89284
  102.2 110.6 %reduce-scatter.2.cloned.1.call-start = ((), (), s32[]{:S(2)}) async-start(), calls=%async_computation.3 | async-start | bytes 1572864 | tf_op jit(solution)/shard_map/reduce_scatter | solution.py:165
  118.8 3.9 %copy-start.4 = (bf16[2048,1024]{1,0:T(8,128)(2,1)S(1)}, bf16[2048,1024]{1,0:T(8,128)(2,1)}, u32[]{:S(2)}) copy-start(bf16[2048,1024]{1,0:T(8,128)(2,1)} %param.22) | copy-start | bytes 12582916
  118.9 4.0 %copy-start.10 = (bf16[256,2048]{1,0:T(8,128)(2,1)S(1)}, bf16[256,2048]{1,0:T(8,128)(2,1)}, u32[]{:S(2)}) copy-start(bf16[256,2048]{1,0:T(8,128)(2,1)} %all-gather.3.cloned.1.call-done) | copy-start | bytes 3145732
  122.9 4.0 %copy-start.9 = (bf16[2048,1024]{1,0:T(8,128)(2,1)S(1)}, bf16[2048,1024]{1,0:T(8,128)(2,1)}, u32[]{:S(2)}) copy-start(bf16[2048,1024]{1,0:T(8,128)(2,1)} %param.21) | copy-start | bytes 12582916
  124.3 21.0 %collective-permute-start = (bf16[2,4,32,1024]{3,2,0,1:T(8,128)(2,1)S(1)}, bf16[2,4,32,1024]{3,2,0,1:T(8,128)(2,1)S(1)}, u32[]{:S(2)}, u32[]{:S(2)}) collective-permute-start(bf16[2,4,32,1024]{3,2,0,1:T(8,128)(2,1)S(1)} %get-tuple-element.9), channel_id=1, source_target_pairs={{0,2},{2,4},{4,6},{6,8},{8,10},{10,12},{12,14},{14,16},{16,18},{18... | collective-permute-start | bytes 1572872 | tf_op jit(solution)/shard_map/ppermute | solution.py:23
  125.6 19.6 %collective-permute-start.1 = (bf16[2,4,32,1024]{3,2,0,1:T(8,128)(2,1)S(1)}, bf16[2,4,32,1024]{3,2,0,1:T(8,128)(2,1)S(1)}, u32[]{:S(2)}, u32[]{:S(2)}) collective-permute-start(bf16[2,4,32,1024]{3,2,0,1:T(8,128)(2,1)S(1)} %get-tuple-element.10), channel_id=1, source_target_pairs={{2,0},{4,2},{6,4},{8,6},{10,8},{12,10},{14,12},{16,14},{18,16},{20... | collective-permute-start | bytes 1572872 | tf_op jit(solution)/shard_map/ppermute | solution.py:25
  154.4 4.4 %slice-start = ((s8[8388608]{0:T(1024)(128)(4,1)}), s8[4194304]{0:T(1024)(128)(4,1)S(1)}, s32[]{:S(2)}) async-start(s8[8388608]{0:T(1024)(128)(4,1)} %bitcast.132), calls=%async_computation.4 | async-start | bytes 8388608
  155.5 4.6 %slice-start.1 = ((s8[8388608]{0:T(1024)(128)(4,1)}), s8[4194304]{0:T(1024)(128)(4,1)S(1)}, s32[]{:S(2)}) async-start(s8[8388608]{0:T(1024)(128)(4,1)} %bitcast.132), calls=%async_computation.5 | async-start | bytes 8388608
  189.1 2.6 %slice-start.2 = ((s8[8388608]{0:T(1024)(128)(4,1)}), s8[4194304]{0:T(1024)(128)(4,1)S(1)}, s32[]{:S(2)}) async-start(s8[8388608]{0:T(1024)(128)(4,1)} %bitcast.134), calls=%async_computation.6 | async-start | bytes 8388608
  189.8 2.9 %slice-start.3 = ((s8[8388608]{0:T(1024)(128)(4,1)}), s8[4194304]{0:T(1024)(128)(4,1)S(1)}, s32[]{:S(2)}) async-start(s8[8388608]{0:T(1024)(128)(4,1)} %bitcast.134), calls=%async_computation.7 | async-start | bytes 8388608
  195.4 3.3 %copy-start.5 = (bf16[256,8,8,128]{3,2,1,0:T(8,128)(2,1)S(1)}, bf16[256,8,8,128]{3,2,1,0:T(8,128)(2,1)}, u32[]{:S(2)}) copy-start(bf16[256,8,8,128]{3,2,1,0:T(8,128)(2,1)} %copy.80) | copy-start | bytes 12582916
  201.2 11.7 %copy-start.2 = (bf16[128,2048]{1,0:T(8,128)(2,1)S(1)}, bf16[128,2048]{1,0:T(8,128)(2,1)}, u32[]{:S(2)}) copy-start(bf16[128,2048]{1,0:T(8,128)(2,1)} %param.13) | copy-start | bytes 1572868
  201.3 13.6 %copy-start.1 = (bf16[128,1024]{1,0:T(8,128)(2,1)S(1)}, bf16[128,1024]{1,0:T(8,128)(2,1)}, u32[]{:S(2)}) copy-start(bf16[128,1024]{1,0:T(8,128)(2,1)} %param.18) | copy-start | bytes 786436
Sparse Core Ops, SparseCore 0:
  95.7 4.9 all-gather.2
  103.4 80.5 all-gather.4
  205.9 6.9 reduce-scatter.1
